TPU v7x, 512 devices: a whole 4x8x8 slice. The times are simulated.
512 devices in a mesh: dp: 4 (over x), kv: 64 (over z, y), tp: 2 (over core).
Axes of the slice: x: 4, y: 8, z: 8, core: 2. Of those that a mesh axis runs over, the one named last changes fastest.
Arguments:
- tokens: bfloat16 [16, 4096], P('dp', ('kv', 'tp')), may hold values from -11 to 11
- attn_gain: float32 [4096], replicated, may hold values from 0.1 to 1.9
- query_weight: bfloat16 [4096, 4096], P('kv', 'tp'), may hold values from -0.09375 to 0.09375
- key_cache: bfloat16 [16, 16384, 2, 128], P('dp', 'kv', 'tp'), may hold values from -820 to 820
- value_cache: bfloat16 [16, 16384, 2, 128], P('dp', 'kv', 'tp'), may hold values from -6 to 6
- head_lambda: float32 [32], P('tp'), may hold values from 0.3 to 0.8
- head_gain: float32 [128], replicated, may hold values from 0.1 to 1.9
- out_weight: bfloat16 [4096, 4096], P('kv', 'tp'), may hold values from -0.09375 to 0.09375
- mlp_gain: float32 [4096], replicated, may hold values from 0.1 to 1.9
- gate_weight: bfloat16 [11264, 4096], P(('kv', 'tp')), may hold values from -0.09375 to 0.09375
- up_weight: bfloat16 [11264, 4096], P(('kv', 'tp')), may hold values from -0.09375 to 0.09375
- down_weight: bfloat16 [11264, 4096], P(('kv', 'tp')), may hold values from -0.21875 to 0.21875
Outputs:
- mixed: bfloat16 [16, 4096], P('dp', ('kv', 'tp'))
All inputs are finite; a program needn't handle non-finite values.
Results may differ from a plain program's by a relative error of at most 0.02.
The roundings to bfloat16 on the way count: a program that leaves them out, or rounds other values in their place, can miss the bound.
Values may be sent and summed in bfloat16 or wider, within the bound.
A program may use at most 64 MiB of HBM per device.

v0:
```python
import jax
import jax.numpy as jnp
from jax import lax
from jax.sharding import Mesh
from jax.sharding import PartitionSpec as P

KV = ("kv_0", "kv_1")
KV_TP = ("kv_0", "kv_1", "tp")


EPS = 1e-06
THETA = 10000.0


def sent_to_all(x, axis):
    copies = jnp.broadcast_to(x, (lax.axis_size(axis), *x.shape))
    return lax.all_to_all(copies, axis, split_axis=0, concat_axis=0, tiled=True)


def joined_along(pieces, dim):
    shape = list(pieces.shape[1:])
    shape[dim] *= pieces.shape[0]
    return jnp.moveaxis(pieces, 0, dim).reshape(shape)


def whole_of(x, axes, dim):
    far, near = axes
    first = sent_to_all(x, far)
    pieces = jnp.swapaxes(sent_to_all(first, near), 0, 1)
    return joined_along(pieces.reshape(-1, *x.shape), dim)


def one_axis_at_a_time(x, axes):
    for axis in axes:
        x = lax.psum(x, axis)
    return x


def collected_together(x, axis):
    leaves = jax.tree.leaves(x)
    turns = sorted(range(len(leaves)), key=lambda k: -leaves[k].size)
    width = (1, *leaves[turns[0]].shape)[-1]
    lines = [
        jnp.pad(leaves[k].reshape(-1), (0, -leaves[k].size % width)).reshape(-1, width)
        for k in turns
    ]
    both, at, found = (lax.all_gather(jnp.concatenate(lines), axis), 0, {})
    for k, line in zip(turns, lines):
        slab = both[:, at : at + len(line)].reshape(len(both), -1)
        found[k] = slab[:, : leaves[k].size].reshape(-1, *leaves[k].shape)
        at += len(line)
    numbers = iter(range(len(leaves)))
    return jax.tree.map(lambda _: found[next(numbers)], x)


def merged_by_axis(x, axes, combine):
    for axis in axes:
        pieces = collected_together(x, axis)
        x = jax.tree.map(lambda part: part[0], pieces)
        for k in range(1, lax.axis_size(axis)):
            x = combine(x, jax.tree.map(lambda part: part[k], pieces))
    return x


def split_up(x, dim, count):
    shape = x.shape
    pieces = x.reshape(*shape[:dim], count, shape[dim] // count, *shape[dim + 1 :])
    return jnp.moveaxis(pieces, dim, 0)


def sum_at_owner(x, axis, dim):
    count = lax.axis_size(axis)
    pieces = lax.all_to_all(split_up(x, dim, count), axis, 0, 0, tiled=True)
    return jnp.sum(pieces, axis=0)


def sum_by_axis(x, axes, dim):
    far, near = axes
    own = sum_at_owner(split_up(x, dim, lax.axis_size(far)), near, dim + 1)
    return jnp.sum(lax.all_to_all(own, far, 0, 0, tiled=True), axis=0)


def rotate(vector, position):
    half_len = vector.shape[-1] // 2
    inv_freq = 1.0 / THETA ** (jnp.arange(half_len, dtype=jnp.float32) / half_len)
    angles = position * inv_freq
    cos_table = jnp.cos(angles)
    sin_table = jnp.sin(angles)
    first_half = vector[..., :half_len]
    second_half = vector[..., half_len:]
    return jnp.concatenate(
        [
            first_half * cos_table - second_half * sin_table,
            second_half * cos_table + first_half * sin_table,
        ],
        axis=-1,
    )


def combine(earlier, latter):
    peak_a, total_a, value_a = earlier
    peak_b, total_b, value_b = latter
    peak_new = jnp.maximum(peak_a, peak_b)
    factor_a = jnp.exp(peak_a - peak_new)
    factor_b = jnp.exp(peak_b - peak_new)
    return (
        peak_new,
        total_a * factor_a + total_b * factor_b,
        value_a * factor_a[..., None] + value_b * factor_b[..., None],
    )


def inner_last(left, right):
    return lax.dot_general(
        left, right, (((1,), (1,)), ((), ())), preferred_element_type=jnp.float32
    )


def shards(
    tokens,
    attn_gain,
    query_weight,
    key_cache,
    value_cache,
    head_lambda,
    head_gain,
    out_weight,
    mlp_gain,
    gate_weight,
    up_weight,
    down_weight,
):
    row_count = tokens.shape[0]
    kv_count = lax.axis_size(KV)
    tp_count = lax.axis_size("tp")
    kv_index = lax.axis_index(KV)
    row_span = query_weight.shape[0]
    full_rows = whole_of(tokens, (("kv_0", "kv_1"), "tp"), 1)
    wide_rows = full_rows.astype(jnp.float32)
    mean_square = jnp.mean(wide_rows * wide_rows, axis=-1, keepdims=True)
    scaled = (wide_rows * attn_gain).astype(jnp.bfloat16)
    local_cols = lax.dynamic_slice_in_dim(scaled, kv_index * row_span, row_span, 1)
    queries = one_axis_at_a_time(
        jnp.dot(local_cols, query_weight, preferred_element_type=jnp.float32), KV
    )
    queries = queries * lax.rsqrt(mean_square + EPS)
    head_count = head_lambda.shape[0]
    kv_local = key_cache.shape[2]
    group_size = head_count // kv_local
    position_count = key_cache.shape[1]
    half_dim = key_cache.shape[3] // 2
    value_dim = value_cache.shape[3]
    queries = queries.reshape(row_count, kv_local, group_size, 2, half_dim)
    rotated = rotate(queries, jnp.float32(position_count * kv_count)).astype(jnp.bfloat16)
    key_grid = key_cache.reshape(row_count, position_count, kv_local, 2, half_dim)
    scores = jnp.einsum(
        "bkgch,bpkch->bkgcp", rotated, key_grid, preferred_element_type=jnp.float32
    ) * half_dim ** (-0.5)
    local_peak = jnp.max(scores, axis=-1)
    weights_exp = jnp.exp(scores - local_peak[..., None])
    lam_grid = head_lambda.reshape(kv_local, group_size)[None, :, :, None]
    exp_total = jnp.sum(weights_exp, axis=-1)
    weighted = jnp.einsum(
        "bkgcp,bpkv->bkgcv",
        weights_exp.astype(jnp.bfloat16),
        value_cache,
        preferred_element_type=jnp.float32,
    )
    peak_all, total_all, weighted_all = merged_by_axis(
        (local_peak, exp_total, weighted), KV, combine
    )
    attended = weighted_all / total_all[..., None]
    difference = attended[:, :, :, 0] - lam_grid * attended[:, :, :, 1]
    head_norm = lax.rsqrt(jnp.mean(difference * difference, axis=-1, keepdims=True) + EPS)
    head_out = (difference * head_norm * head_gain).reshape(row_count, head_count * value_dim)
    head_out = head_out.astype(jnp.bfloat16)
    out_part = inner_last(head_out, out_weight).astype(jnp.bfloat16)
    pieces = whole_of(out_part, (("kv_0", "kv_1"), "tp"), 1)
    attention = jnp.sum(
        pieces.astype(jnp.float32).reshape(row_count, kv_count, tp_count, -1), axis=2
    )
    stream = wide_rows + attention.reshape(row_count, -1)
    stream_square = jnp.mean(stream * stream, axis=-1, keepdims=True)
    normed = (stream * lax.rsqrt(stream_square + EPS) * mlp_gain).astype(jnp.bfloat16)
    gate_out = inner_last(normed, gate_weight)
    up_out = inner_last(normed, up_weight)
    hidden = (jax.nn.silu(gate_out) * up_out).astype(jnp.bfloat16)
    own_cols = tokens.shape[1]
    down_cols = sum_by_axis(
        lax.dot_general(
            down_weight, hidden, (((0,), (1,)), ((), ())), preferred_element_type=jnp.float32
        ),
        (("kv_0", "kv_1"), "tp"),
        0,
    )
    column_index = lax.axis_index(KV_TP)
    own_stream = lax.dynamic_slice_in_dim(stream, column_index * own_cols, own_cols, 1)
    return (own_stream + down_cols.T).astype(jnp.bfloat16)


def solution(mesh):
    torus = Mesh(
        mesh.devices.reshape(mesh.shape["dp"], 8, 8, mesh.shape["tp"]), ("dp", "kv_0", "kv_1", "tp")
    )
    in_specs = (
        P("dp", KV_TP),
        P(),
        P(KV, "tp"),
        P("dp", KV, "tp", None),
        P("dp", KV, "tp", None),
        P("tp"),
        P(),
        P(KV, "tp"),
        P(),
        P(KV_TP, None),
        P(KV_TP, None),
        P(KV_TP, None),
    )
    out_specs = P("dp", KV_TP)
    return jax.shard_map(
        shards, mesh=torus, in_specs=in_specs, out_specs=out_specs, check_vma=False
    )
```

profile of v0, /device:TPU:1, one launch (start us, length us, event | category | flops | bytes accessed | tf_op | source)
XLA Modules:
  0.0 199.4 jit_solution(2808983307863396402)
XLA Ops:
  0.0 1.4 broadcast_in_dim.8
  1.4 17.3 %all-to-all-start = ((bf16[64,4,32]{2,1,0:T(4,128)(2,1)}), bf16[64,4,32]{2,1,0:T(4,128)(2,1)S(1)}, u32[]{:S(2)}, u32[]{:S(2)}) async-start(bf16[64,4,32]{2,1,0:T(4,128)(2,1)} %broadcast_in_dim.8), calls=%async_computation | async-start | bytes 131072 | tf_op jit(solution)/shard_map/all_to_all | solution.py:17
  18.8 1.1 copy.28
  19.9 0.8 dynamic-slice
  20.7 9.1 %all-to-all-done = bf16[64,4,32]{2,1,0:T(4,128)(2,1)S(1)} async-done(((bf16[64,4,32]{2,1,0:T(4,128)(2,1)}), bf16[64,4,32]{2,1,0:T(4,128)(2,1)S(1)}, u32[]{:S(2)}, u32[]{:S(2)}) %all-to-all-start) | async-done | bytes 16416 | tf_op jit(solution)/shard_map/all_to_all | solution.py:17
  29.9 0.1 reshape.2089
  30.0 5.5 %all_to_all.30 = bf16[2,2,4096]{2,1,0:T(2,128)(2,1)S(1)} all-to-all(bf16[2,2,4096]{2,1,0:T(2,128)(2,1)S(1)} %reshape.2089), channel_id=1, replica_groups=mesh['dp'=4,'kv_0'=8,'kv_1'=8,'tp'=2] {'tp'}, dimensions={0} | all-to-all | bytes 65536 | tf_op jit(solution)/shard_map/all_to_all | solution.py:17
  35.6 0.2 copy.25
  35.8 0.2 reshape.1988
  35.9 0.1 multiply_reduce_fusion.1
  36.1 0.7 copy-done.4
  36.7 0.2 fusion.48
  36.9 20.3 %psum.14 = f32[4,2048]{1,0:T(4,128)S(1)} all-reduce(f32[4,2048]{1,0:T(4,128)S(1)} %fusion.48), channel_id=1, replica_groups=mesh['dp'=4,'kv_0'=8,'kv_1'=8,'tp'=2] {'kv_0'}, use_global_device_ids=true, to_apply=%region_0.0 | all-reduce | flops 8192 | bytes 65536 | tf_op jit(solution)/shard_map/psum | solution.py:35
  57.2 20.5 %psum.15 = f32[4,2048]{1,0:T(4,128)S(1)} all-reduce(f32[4,2048]{1,0:T(4,128)S(1)} %psum.14), channel_id=1, replica_groups=mesh['dp'=4,'kv_0'=8,'kv_1'=8,'tp'=2] {'kv_1'}, use_global_device_ids=true, to_apply=%region_1.0 | all-reduce | flops 8192 | bytes 65536 | tf_op jit(solution)/shard_map/psum | solution.py:35
  78.0 0.1 fusion.99
  78.1 0.3 fusion.100
  78.6 0.2 fusion.4
  78.8 0.1 reshape.1986
  79.0 0.1 reshape.1985
  79.1 0.2 fusion.2
  79.4 18.9 %all-gather.2 = f32[8,130,128]{2,1,0:T(8,128)S(1)} all-gather(f32[1,130,128]{2,1,0:T(8,128)S(1)} %maximum_bitcast_fusion), channel_id=2, replica_groups=mesh['dp'=4,'kv_0'=8,'kv_1'=8,'tp'=2] {'kv_0'}, dimensions={0}, use_global_device_ids=true | all-gather | bytes 599040 | tf_op jit(solution)/shard_map/all_gather | solution.py:47
  98.5 0.3 fusion.9
  98.8 19.4 %all-gather.3 = f32[8,130,128]{2,1,0:T(8,128)S(1)} all-gather(f32[1,130,128]{2,1,0:T(8,128)S(1)} %maximum_bitcast_fusion.1), channel_id=3, replica_groups=mesh['dp'=4,'kv_0'=8,'kv_1'=8,'tp'=2] {'kv_1'}, dimensions={0}, use_global_device_ids=true | all-gather | bytes 599040 | tf_op jit(solution)/shard_map/all_gather | solution.py:47
  118.3 0.1 squeeze.225
  118.4 0.1 squeeze.224
  118.6 0.1 squeeze.223
  118.7 0.1 squeeze.222
  118.8 0.1 squeeze.221
  119.0 0.1 squeeze.220
  119.1 0.1 squeeze.219
  119.3 0.1 squeeze.218
  119.4 0.1 squeeze.203
  119.5 0.1 squeeze.212
  119.7 0.1 squeeze.210
  119.8 0.1 squeeze.208
  120.0 0.1 squeeze.206
  120.1 0.1 squeeze.204
  120.3 0.1 squeeze.214
  120.4 0.1 squeeze.216
  120.7 1.2 add_divide_fusion
  122.0 0.2 multiply_reduce_fusion.2
  122.3 0.6 copy-done.5
  122.8 0.2 convolution_convert_fusion
  123.2 17.5 %all_to_all.31 = bf16[64,2,128]{2,1,0:T(2,128)(2,1)S(1)} all-to-all(bf16[64,2,128]{2,1,0:T(2,128)(2,1)S(1)} %reshape.2091), channel_id=1, replica_groups=mesh['dp'=4,'kv_0'=8,'kv_1'=8,'tp'=2] {'kv_0','kv_1'}, dimensions={0} | all-to-all | bytes 65536 | tf_op jit(solution)/shard_map/all_to_all | solution.py:17
  140.8 0.2 reshape.2093
  141.0 31.9 %all_to_all.32 = bf16[2,2,8192]{2,1,0:T(2,128)(2,1)S(1)} all-to-all(bf16[2,2,8192]{2,1,0:T(2,128)(2,1)S(1)} %reshape.2093), channel_id=1, replica_groups=mesh['dp'=4,'kv_0'=8,'kv_1'=8,'tp'=2] {'tp'}, dimensions={0} | all-to-all | bytes 131072 | tf_op jit(solution)/shard_map/all_to_all | solution.py:17
  172.9 0.1 reshape.2094
  173.1 0.4 bitcast_reduce_fusion
  173.8 0.1 multiply_reduce_fusion
  173.9 0.7 copy-done.1
  174.6 0.3 fusion.95
  174.9 0.7 convolution_bitcast_fusion
  175.7 0.3 reshape_reshape.2
  176.0 0.1 copy.35
  176.1 0.1 reshape.2095
  176.2 3.8 %all_to_all.33 = f32[2,1,8192]{2,1,0:T(1,128)S(1)} all-to-all(f32[2,1,8192]{2,1,0:T(1,128)S(1)} %reshape.2095), channel_id=1, replica_groups=mesh['dp'=4,'kv_0'=8,'kv_1'=8,'tp'=2] {'tp'}, dimensions={0} | all-to-all | bytes 131072 | tf_op jit(solution)/shard_map/all_to_all | solution.py:73
  180.0 0.5 broadcast.362
  180.5 0.8 reduce.224
  181.4 0.1 reshape.2096
  181.6 0.7 reshape.2097
  182.4 4.6 %all-to-all-start.5 = ((f32[64,1,128]{2,1,0:T(1,128)}), f32[64,1,128]{2,1,0:T(1,128)S(1)}, u32[]{:S(2)}, u32[]{:S(2)}) async-start(f32[64,1,128]{2,1,0:T(1,128)} %reshape.2097), calls=%async_computation.5 | async-start | bytes 65536 | tf_op jit(solution)/shard_map/all_to_all | solution.py:80
  187.0 10.8 %all-to-all-done.5 = f32[64,1,128]{2,1,0:T(1,128)S(1)} async-done(((f32[64,1,128]{2,1,0:T(1,128)}), f32[64,1,128]{2,1,0:T(1,128)S(1)}, u32[]{:S(2)}, u32[]{:S(2)}) %all-to-all-start.5) | async-done | bytes 32800 | tf_op jit(solution)/shard_map/all_to_all | solution.py:80
  197.8 0.7 reduce.225
  198.8 0.6 fusion.44
  (56 shorter events, 2.1 us)
Async XLA Ops:
  0.0 174.9 %copy-start = (bf16[88,4096]{1,0:T(8,128)(2,1)S(1)}, bf16[88,4096]{1,0:T(8,128)(2,1)}, u32[]{:S(2)}) copy-start(bf16[88,4096]{1,0:T(8,128)(2,1)} %param.23) | copy-start | bytes 2162692
  1.4 17.3 %copy-start.7 = (f32[16]{0:T(128)S(1)}, f32[16]{0:T(128)}, u32[]{:S(2)}) copy-start(f32[16]{0:T(128)} %param.17) | copy-start | bytes 196
  1.4 17.3 %copy-start.8 = (f32[128]{0:T(128)S(1)}, f32[128]{0:T(128)}, u32[]{:S(2)}) copy-start(f32[128]{0:T(128)} %param.18) | copy-start | bytes 1540
  1.4 28.3 %all-to-all-start = ((bf16[64,4,32]{2,1,0:T(4,128)(2,1)}), bf16[64,4,32]{2,1,0:T(4,128)(2,1)S(1)}, u32[]{:S(2)}, u32[]{:S(2)}) async-start(bf16[64,4,32]{2,1,0:T(4,128)(2,1)} %broadcast_in_dim.8), calls=%async_computation | async-start | bytes 131072 | tf_op jit(solution)/shard_map/all_to_all | solution.py:17
  35.8 1.0 copy-start.4
  78.1 1.0 copy-start.3
  121.9 1.0 copy-start.5
  173.5 1.1 copy-start.1
  173.6 1.0 copy-start.6
  173.7 1.2 copy-start.2
  182.4 15.5 %all-to-all-start.5 = ((f32[64,1,128]{2,1,0:T(1,128)}), f32[64,1,128]{2,1,0:T(1,128)S(1)}, u32[]{:S(2)}, u32[]{:S(2)}) async-start(f32[64,1,128]{2,1,0:T(1,128)} %reshape.2097), calls=%async_computation.5 | async-start | bytes 65536 | tf_op jit(solution)/shard_map/all_to_all | solution.py:80
where the time goes:
time: 200 us; the launch traced here: 199 us
  blocking collectives  138 us (69%)
  starting transfers between devices  21.9 us (11%)
  waiting for transfers between devices  19.9 us (10%)
  local copies, waits for them, and re-layouts  12 us (6%)
  other arithmetic  5.28 us (3%)
    all_to_all x3, blocking collectives, sent_to_all(): return lax.all_to_all(copies, axis, split_axis=0, concat_axis=0, tiled=True)  54.9 us
    psum x2, blocking collectives, one_axis_at_a_time(): x = lax.psum(x, axis)  40.8 us
    all_gather x2, blocking collectives, collected_together(): both, at, found = (lax.all_gather(jnp.concatenate(lines), axis), 0, {})  38.3 us
    all_to_all x1, starting transfers between devices, sent_to_all(): return lax.all_to_all(copies, axis, split_axis=0, concat_axis=0, tiled=True)  17.3 us
    all_to_all x1, waiting for transfers between devices, sum_by_axis(): return jnp.sum(lax.all_to_all(own, far, 0, 0, tiled=True), axis=0)  10.8 us
    all_to_all x1, waiting for transfers between devices, sent_to_all(): return lax.all_to_all(copies, axis, split_axis=0, concat_axis=0, tiled=True)  9.06 us
    unnamed x32, local copies, waits for them, and re-layouts  5 us
    all_to_all x1, starting transfers between devices, sum_by_axis(): return jnp.sum(lax.all_to_all(own, far, 0, 0, tiled=True), axis=0)  4.61 us
  transfers between devices with their start and end apart: 2, of which 2 were waited for; matrix products, arithmetic and copies ran while one was open for 1% of the time, Pallas kernels for 0%

commit v1 on v0

v1 whole, which is shorter than its diff:
```python
import functools

import jax
import jax.numpy as jnp
import numpy as np
from jax import lax
from jax.experimental import pallas as pl
from jax.experimental.pallas import tpu as pltpu
from jax.sharding import Mesh
from jax.sharding import PartitionSpec as P

KV = ("kv_0", "kv_1")
KV_TP = ("kv_0", "kv_1", "tp")
AXES = ("dp", "kv_0", "kv_1", "tp")
MESH = pl.DeviceIdType.MESH
EPS = 1e-06
THETA = 10000.0
F32 = jnp.float32
BF16 = jnp.bfloat16
N = 8
FAR_FIRST = (4, 3, 5, 2, 6, 1, 7, 0)
RING = FAR_FIRST[:7]
PLANE = [(a, b) for a in FAR_FIRST for b in FAR_FIRST if a or b]
OTHERS = [(a, b, c) for a in FAR_FIRST for b in FAR_FIRST for c in (1, 0) if a or b or c]


def iota(shape, dim):
    return lax.broadcasted_iota(jnp.int32, shape, dim)


def contract_last(left, right):
    return lax.dot_general(left, right, (((1,), (1,)), ((), ())), preferred_element_type=F32)


def rounded(x):
    return x.astype(BF16).astype(F32)


def kernel(
    tok_h, ag_h, wq_h, k_h, v_h, lam_h, hg_h, wo_h, mg_h, wg_h, wu_h, wd_h, rope_h,
    out_ref,
    tok, ag, wq, kc, vc, lam, hg, wo, mg, wg, wu, wd, rope,
    tokx, wox, qs, qr, qz, qzr, qa, ss, sr, hb, sf, gs, gr, gf, qp,
    lsem, psem, ssem, rsem,
):
    d, z, y, t = (lax.axis_index(a) for a in AXES)
    kv = z * N + y
    dev = kv * 2 + t
    owned = y * N + z

    def at(dz, dy, dt):
        return (d, lax.rem(z + dz, N), lax.rem(y + dy, N), lax.rem(t + dt, 2))

    barrier = pltpu.get_barrier_semaphore()
    near = [(0, k, 0) for k in RING] + [(k, 0, 0) for k in RING] + [(0, 0, 1)]
    for p in near:
        pl.semaphore_signal(barrier, inc=1, device_id=at(*p), device_id_type=MESH)

    pairs = (
        (tok_h, tok), (ag_h, ag), (wq_h, wq), (mg_h, mg), (rope_h, rope), (wo_h, wo), (k_h, kc),
        (v_h, vc), (lam_h, lam), (hg_h, hg), (wg_h, wg), (wu_h, wu), (wd_h, wd),
    )
    loads = {}
    for k, (src, dst) in enumerate(pairs):
        loads[k] = pltpu.make_async_copy(src, dst, lsem.at[k])
        loads[k].start()

    def remote(src, dst, k, p):
        return pltpu.make_async_remote_copy(
            src_ref=src, dst_ref=dst, send_sem=ssem.at[k], recv_sem=rsem.at[k],
            device_id=at(*p), device_id_type=MESH,
        )

    row8 = iota((8, 128), 0)
    lane8 = iota((8, 128), 1)

    loads[0].wait()
    loads[1].wait()
    loads[2].wait()
    gain_row = jnp.broadcast_to(ag[pl.ds(dev // 4, 1), :], (8, 128))

    def gain_of(index):
        return pltpu.roll(gain_row, lax.rem(128 - 32 * lax.rem(index, 4), 128), 1)[:, :32]

    def twice(x):
        wide = x.astype(F32)
        return jnp.concatenate([wide, wide], axis=0)

    own8 = twice(tok[...])
    half = pl.multiple_of(t * 32, 32)
    rest = pl.multiple_of((1 - t) * 32, 32)
    qp[...] = jnp.dot((own8 * gain_of(dev)).astype(BF16), wq[pl.ds(half, 32), :], preferred_element_type=F32)
    own_square = jnp.sum(own8 * own8, axis=1, keepdims=True)
    other_gain = gain_of(dev + 1 - 2 * t)

    loads[3].wait()
    for v in range(16):
        two = jnp.where(row8 < 4, mg[2 * v : 2 * v + 1, :], mg[2 * v + 1 : 2 * v + 2, :])
        kept = jnp.where(lane8 // 32 == row8 % 4, two, 0.0)
        full = kept + pltpu.roll(kept, 32, 1)
        gf[8 * v : 8 * v + 8, :] = full + pltpu.roll(full, 64, 1)

    pl.semaphore_wait(barrier, len(near))

    remote(tok, tokx, 0, (0, 0, 1)).start()
    remote(tok, tokx, 0, (0, 0, 1)).wait_recv()
    other8 = twice(tokx[...])
    queries = qp[...] + jnp.dot(
        (other8 * other_gain).astype(BF16), wq[pl.ds(rest, 32), :], preferred_element_type=F32
    )
    square = jnp.broadcast_to(
        own_square + jnp.sum(other8 * other8, axis=1, keepdims=True), (8, 128)
    )
    for j in range(N):
        left = queries[:, 256 * j : 256 * j + 128]
        right = queries[:, 256 * j + 128 : 256 * j + 256]
        qs[j, 0:8, :] = jnp.where(row8 < 4, left, right)
        qs[j, 8:16, :] = square
    for k in RING:
        remote(qs.at[lax.rem(y + k, N)], qr.at[k - 1], 1, (0, k, 0)).start()

    loads[5].wait()
    remote(wo.at[pl.ds(rest, 32), :], wox, 2, (0, 0, 1)).start()

    remote(qr, qr, 1, (0, 1, 0)).wait_recv()
    qz[...] = jnp.sum(qr[...], axis=0) + qs[y]
    for k in RING:
        remote(qz, qzr.at[k - 1], 3, (k, 0, 0)).start()
    loads[4].wait()
    remote(qzr, qzr, 3, (1, 0, 0)).wait_recv()
    total = jnp.sum(qzr[...], axis=0) + qz[...]
    mean_square = total[8:16] * (1.0 / 4096.0)
    query = total[0:8] * lax.rsqrt(mean_square + EPS)
    swapped = jnp.where(lane8 % 64 < 32, pltpu.roll(query, 96, 1), pltpu.roll(query, 32, 1))
    qa[y] = rounded(query * rope[0] + swapped * rope[1])
    for k in RING:
        remote(qa.at[y], qa.at[y], 4, (0, k, 0)).start()
    loads[6].wait()
    loads[7].wait()
    remote(qa.at[0:7], qa.at[0:7], 4, (0, 1, 0)).wait_recv()

    rotated = qa[...].reshape(64, 128)
    low = iota((64, 128), 1) < 64
    both = jnp.concatenate(
        [jnp.where(low, rotated, 0.0), jnp.where(low, 0.0, rotated)], axis=0
    ).astype(BF16)
    sequence = iota((128, 256), 0) % 4
    scores = contract_last(both, kc[0])
    for b in range(1, 4):
        scores = jnp.where(sequence == b, contract_last(both, kc[b]), scores)
    scores = scores * 0.125
    peak = jnp.max(scores, axis=1, keepdims=True)
    raised = jnp.exp(scores - peak)
    mass = jnp.sum(raised, axis=1, keepdims=True)
    probs = raised.astype(BF16)
    sequence_v = iota((128, 128), 0) % 4
    weighted = jnp.dot(probs, vc[0], preferred_element_type=F32)
    for b in range(1, 4):
        weighted = jnp.where(
            sequence_v == b, jnp.dot(probs, vc[b], preferred_element_type=F32), weighted
        )
    lane64 = iota((64, 128), 1)
    ss[0] = weighted[:64]
    ss[1] = weighted[64:]
    ss[2] = jnp.where(
        lane64 == 0, peak[:64],
        jnp.where(lane64 == 1, peak[64:], jnp.where(lane64 == 2, mass[:64], mass[64:])),
    )
    for p in PLANE:
        to = lax.rem(y + p[1], N) * N + lax.rem(z + p[0], N)
        remote(ss.at[:, pl.ds(to, 1), :], sr.at[:, pl.ds(owned, 1), :], 5, (*p, 0)).start()
    for k in range(3):
        sr[k, pl.ds(owned, 1), :] = ss[k, pl.ds(owned, 1), :]
    loads[8].wait()
    loads[9].wait()
    remote(ss.at[:, 0:63, :], sr.at[:, 0:63, :], 5, (0, 1, 0)).wait_recv()

    marks = sr[2]

    def attended(c):
        peaks = marks[:, c : c + 1]
        factor = jnp.exp(peaks - jnp.max(peaks, axis=0, keepdims=True))
        whole = jnp.sum(marks[:, c + 2 : c + 3] * factor, axis=0, keepdims=True)
        return jnp.sum(sr[c] * factor, axis=0, keepdims=True) / whole

    head = 2 * y + z // 4
    difference = attended(0) - lam[head] * attended(1)
    head_norm = lax.rsqrt(jnp.mean(difference * difference, axis=1, keepdims=True) + EPS)
    hb[t, pl.ds(owned, 1), :] = rounded(difference * head_norm * hg[...])
    spot = hb.at[t, pl.ds(owned, 1), :]
    for p in OTHERS:
        remote(spot, spot, 6, p).start()
    remote(wox, wox, 2, (0, 0, 1)).wait_recv()
    remote(sf.at[0:127], sf.at[0:127], 6, (0, 1, 0)).wait_recv()

    def projected(group, weight):
        heads = hb[group]
        tiles = []
        for j in range(N):
            tile = heads[8 * j : 8 * j + 8]
            tiles += [jnp.where(row8 < 4, tile, 0.0), jnp.where(row8 < 4, 0.0, tile)]
        product = contract_last(jnp.concatenate(tiles, axis=1).astype(BF16), weight)
        return rounded(product[0:4] + product[4:8])

    part = projected(t, wo[pl.ds(half, 32), :]) + projected(1 - t, wox[...])
    stream = tok[...].astype(F32) + part
    line = jnp.concatenate([stream[b : b + 1] for b in range(4)], axis=1)
    sf[pl.ds(dev, 1), :] = line
    spot_f = sf.at[pl.ds(dev, 1), :]
    for p in OTHERS:
        remote(spot_f, spot_f, 7, p).start()
    loads[10].wait()
    loads[11].wait()
    loads[12].wait()
    remote(sf.at[0:127], sf.at[0:127], 7, (0, 1, 0)).wait_recv()

    rows = sf[...]
    squares = jnp.sum(rows * rows, axis=0, keepdims=True)
    group1 = iota((1, 128), 1) // 32
    scale = jnp.zeros((1, 128), F32)
    for b in range(4):
        mine = group1 == b
        whole = jnp.sum(jnp.where(mine, squares, 0.0), axis=1, keepdims=True)
        scale = jnp.where(mine, lax.rsqrt(whole * (1.0 / 4096.0) + EPS), scale)
    normed = rounded(rows * scale * gf[...])
    diagonal = iota((128, 128), 1) // 32 == iota((128, 128), 0) % 4
    lefts = []
    for s in range(4):
        moved = normed if s == 0 else pltpu.roll(normed, 32 * s, 1)
        kept = jnp.where(diagonal, moved, 0.0)
        tiles = []
        for v in range(16):
            tile = kept[8 * v : 8 * v + 8]
            tiles += [jnp.where(row8 < 4, tile, 0.0), jnp.where(row8 < 4, 0.0, tile)]
        lefts.append(jnp.concatenate(tiles, axis=1))
    left = jnp.concatenate(lefts, axis=0).astype(BF16)

    def folded(product):
        result = None
        for s in range(4):
            block = product[8 * s : 8 * s + 8]
            block = block + jnp.concatenate([block[4:8], block[0:4]], axis=0)
            if s:
                block = jnp.concatenate([block[s:8], block[0:s]], axis=0)
            result = block if result is None else result + block
        return result

    gate = folded(contract_last(left, wg[...]))
    up = folded(contract_last(left, wu[...]))
    hidden = gate / (1.0 + jnp.exp(-gate)) * up
    turned = [hidden] + [jnp.concatenate([hidden[s:8], hidden[0:s]], axis=0) for s in range(1, 4)]
    down = jnp.dot(
        jnp.concatenate(turned, axis=0).astype(BF16), wd[...], preferred_element_type=F32
    )
    for v in range(16):
        result = None
        for s in range(4):
            even = down[8 * s : 8 * s + 8, 256 * v : 256 * v + 128]
            odd = down[8 * s : 8 * s + 8, 256 * v + 128 : 256 * v + 256]
            tile = jnp.where(row8 < 4, even, odd)
            if s == 0:
                result = tile
            else:
                place = lane8 // 32 == lax.rem(row8 + s, 4)
                result = jnp.where(place, pltpu.roll(tile, 32 * s, 1), result)
        gs[8 * v : 8 * v + 8, :] = result
    for p in OTHERS:
        _, pz, py, pt = at(*p)
        to = (pz * N + py) * 2 + pt
        remote(gs.at[pl.ds(to, 1), :], gr.at[pl.ds(dev, 1), :], 8, p).start()
    gr[pl.ds(dev, 1), :] = gs[pl.ds(dev, 1), :]
    mine = sf[pl.ds(dev, 1), :]
    remote(gr.at[0:127], gr.at[0:127], 8, (0, 1, 0)).wait_recv()
    out_ref[...] = mine + jnp.sum(gr[...], axis=0, keepdims=True)

    for k, ref in (
        (0, tok), (1, qr), (2, wox), (3, qzr), (4, qa.at[0:7]), (5, sr.at[:, 0:63, :]),
        (6, sf.at[0:127]), (7, sf.at[0:127]), (8, gr.at[0:127]),
    ):
        remote(ref, ref, k, (0, 1, 0)).wait_send()


def rope_tables():
    half = 32
    rate = (1.0 / np.float32(THETA) ** (np.arange(half, dtype=np.float32) / np.float32(half))).astype(np.float32)
    angle = (np.float32(16384) * rate).astype(np.float32).astype(np.float64)
    cos, sin = np.cos(angle).astype(np.float32), np.sin(angle).astype(np.float32)
    table = np.stack([np.tile(cos, 4), np.concatenate([-sin, sin, -sin, sin])])
    return np.ascontiguousarray(np.broadcast_to(table[:, None, :], (2, 8, 128)))


def shards(tokens, attn_gain, query_weight, key_cache, value_cache, head_lambda, head_gain,
           out_weight, mlp_gain, gate_weight, up_weight, down_weight):
    args = (
        tokens, attn_gain.reshape(32, 128), query_weight, key_cache.reshape(4, 256, 128),
        value_cache.reshape(4, 256, 128), head_lambda, head_gain.reshape(1, 128), out_weight,
        mlp_gain.reshape(32, 128), gate_weight, up_weight, down_weight, jnp.asarray(rope_tables()),
    )
    local = [
        pltpu.SMEM(a.shape, a.dtype) if k == 5 else pltpu.VMEM(a.shape, a.dtype)
        for k, a in enumerate(args)
    ]
    wide = lambda *shape: pltpu.VMEM(shape, F32)
    line = pl.pallas_call(
        kernel,
        out_shape=jax.ShapeDtypeStruct((1, 128), F32),
        in_specs=[pl.BlockSpec(memory_space=pl.ANY)] * len(args),
        out_specs=pl.BlockSpec(memory_space=pltpu.VMEM),
        scratch_shapes=local + [
            pltpu.VMEM((4, 32), BF16), pltpu.VMEM((32, 2048), BF16),
            wide(8, 16, 128), wide(7, 16, 128), wide(16, 128), wide(7, 16, 128), wide(8, 8, 128),
            wide(3, 64, 128), wide(3, 64, 128), wide(2, 64, 128), wide(128, 128),
            wide(128, 128), wide(128, 128), wide(128, 128), wide(8, 2048),
            pltpu.SemaphoreType.DMA((13,)), pltpu.SemaphoreType.DMA((1,)),
            pltpu.SemaphoreType.DMA((9,)), pltpu.SemaphoreType.DMA((9,)),
        ],
        compiler_params=pltpu.CompilerParams(collective_id=0, has_side_effects=True),
    )(*args)
    return line.reshape(4, 32).astype(BF16)


def solution(mesh):
    torus = Mesh(mesh.devices.reshape(mesh.shape["dp"], 8, 8, mesh.shape["tp"]), AXES)
    in_specs = (
        P("dp", KV_TP), P(), P(KV, "tp"), P("dp", KV, "tp", None), P("dp", KV, "tp", None),
        P("tp"), P(), P(KV, "tp"), P(), P(KV_TP, None), P(KV_TP, None), P(KV_TP, None),
    )
    return jax.shard_map(
        shards, mesh=torus, in_specs=in_specs, out_specs=P("dp", KV_TP), check_vma=False
    )
```

time: 200 us -> 60.9 us (0.30)
  blocking collectives: 138 us -> 0 us
  Pallas kernels: 0 us -> 59.4 us
  starting transfers between devices: 21.9 us -> 0 us
  waiting for transfers between devices: 19.9 us -> 0 us
  local copies, waits for them, and re-layouts: 12 us -> 0.65 us
  other arithmetic: 5.28 us -> 0.7 us
    pallas_call x0 -> x1, Pallas kernels: none -> 59.4 us  [shards(): pl.pallas_call(kernel, out_shape=jax.ShapeDtypeStruct((1, 128), F32), in_...]
    all_to_all x4 -> x0, blocking collectives: 58.7 us -> none  [the longest x3 54.9 us: sent_to_all(): return lax.all_to_all(copies, axis, split_axis=0, concat_axis=0, tiled=True)]
    psum x2 -> x0, blocking collectives: 40.8 us -> none  [one_axis_at_a_time(): x = lax.psum(x, axis)]
    all_gather x2 -> x0, blocking collectives: 38.3 us -> none  [collected_together(): both, at, found = (lax.all_gather(jnp.concatenate(lines), axis), 0, {})]
    all_to_all x2 -> x0, starting transfers between devices: 21.9 us -> none  [the longest x1 17.3 us: sent_to_all(): return lax.all_to_all(copies, axis, split_axis=0, concat_axis=0, tiled=True)]
    all_to_all x2 -> x0, waiting for transfers between devices: 19.9 us -> none  [the longest x1 10.8 us: sum_by_axis(): return jnp.sum(lax.all_to_all(own, far, 0, 0, tiled=True), axis=0)]
    unnamed x32 -> x0, local copies, waits for them, and re-layouts: 5 us -> none
    squeeze x16 -> x0, local copies, waits for them, and re-layouts: 2.13 us -> none  [the longest x14 1.86 us: merged_by_axis(): x = combine(x, jax.tree.map(lambda part: part[k], pieces))]
  transfers between devices with their start and end apart: 2 -> 0, of which waited for: 2 -> 0; matrix products, arithmetic and copies ran while one was open for 1% -> 0% of each run, Pallas kernels for 0% -> 0%
where the time goes in v1:
time: 60.9 us; the launch traced here: 60.8 us
  Pallas kernels  59.4 us (98%)
  other arithmetic  0.7 us (1%)
  local copies, waits for them, and re-layouts  0.65 us (1%)
    pallas_call x1, Pallas kernels, shards(): pl.pallas_call(kernel, out_shape=jax.ShapeDtypeStruct((1, 128), F32), in_...  59.4 us

profile of v1, /device:TPU:1, one launch (start us, length us, event | category | flops | bytes accessed | tf_op | source)
XLA Modules:
  0.0 60.8 jit_solution(989577447349510566)
XLA Ops:
  0.0 59.4 %shard_map.127 = f32[1,128]{1,0:T(1,128)} custom-call(bf16[4,32]{1,0:T(4,128)(2,1)} %tok_h.1, f32[32,128]{1,0:T(8,128)} %bitcast.7, bf16[64,2048]{1,0:T(8,128)(2,1)} %wq_h.1, bf16[4,256,128]{2,1,0:T(8,128)(2,1)} %bitcast.5, bf16[4,256,128]{2,1,0:T(8,128)(2,1)} %bitcast.6, f32[16]{0:T(128)} %lam_h.1, f32[1,128]{1,0:T(1,128)} %bitcast.9, ...), custom_call_target="tpu_custom_call" | custom-call | tf_op jit(solution)/shard_map/pallas_call | solution.py:304
  59.4 0.7 %convert_reduce_fusion = bf16[128]{0:T(256)(128)(2,1)S(1)} fusion(f32[1,128]{1,0:T(1,128)} %shard_map.127), kind=kLoop, calls=%fused_computation | loop fusion | flops 128 | bytes 768 | tf_op jit(solution)/shard_map/convert_element_type | solution.py:319
  60.1 0.6 %convert_element_type.7 = bf16[4,32]{1,0:T(4,128)(2,1)} reshape(bf16[128]{0:T(256)(128)(2,1)S(1)} %convert_reduce_fusion) | data formatting | bytes 512 | tf_op jit(solution)/shard_map/convert_element_type | solution.py:319
